TPU v7x, 32 devices: a whole 2x2x4 slice. The times are simulated.
32 devices in a mesh: sp: 16 (over z, x, core), tp: 2 (over y).
Axes of the slice: x: 2, y: 2, z: 4, core: 2. Of those that a mesh axis runs over, the one named last changes fastest.
Arguments:
- residual: bfloat16 [4096, 2048], P(('sp', 'tp')), may hold values from -6 to 6
- query_vectors: bfloat16 [4096, 512], P('sp', 'tp'), may hold values from -6 to 6
- key_vectors: bfloat16 [4096, 512], P('sp', 'tp'), may hold values from -6 to 6
- value_vectors: bfloat16 [4096, 512], P('sp', 'tp'), may hold values from -6 to 6
- in_gate: float32 [8, 4096], P('tp', 'sp'), may hold values from -9 to 190
- forget_gate: float32 [8, 4096], P('tp', 'sp'), may hold values from -1 to 12
- documents: int32 [4096], P('sp'), may hold values from 0 to 3, never falling along the last dimension, each value on 1 to 2048 neighbouring positions
- w_out: bfloat16 [512, 2048], P('tp'), may hold values from -0.25 to 0.25
- norm_gain: bfloat16 [2048], replicated, may hold values from 0.099609375 to 1.8984375
- w_up: bfloat16 [2048, 8192], P('sp', 'tp'), may hold values from -0.125 to 0.125
- w_down: bfloat16 [8192, 2048], P('tp', 'sp'), may hold values from -0.0625 to 0.0625
Outputs:
- layer_out: bfloat16 [4096, 2048], P(('sp', 'tp'))
Inputs may be any that keep to these rules, and one draw needn't show every extreme that they name: `documents`: document numbers never fall along the positions; every document has 1 to 2048 positions.
All inputs are finite; a program needn't handle non-finite values.
Results may differ from a plain program's by a relative error of at most 0.015.
Values may be sent and summed in bfloat16 or wider, within the bound.
A program may use at most 128 MiB of HBM per device.

v0:
```python
import jax
import jax.numpy as jnp
from jax import lax
from jax.sharding import PartitionSpec as P

SPAN = 128
very_negative = -1e30
epsilon = 1e-06


def carried_in(value, axis, combine, identity):
    length, here = (lax.axis_size(axis), lax.axis_index(axis))
    everything = jax.tree.map(lambda part: lax.all_gather(part, axis), value)
    start = jax.tree.map(
        lambda part, zero: jnp.broadcast_to(jnp.asarray(zero, part.dtype), part.shape),
        value,
        identity,
    )

    def lap(k, before):
        reached = k < here
        new = combine(before, jax.tree.map(lambda part: part[k], everything))
        return jax.tree.map(lambda a, b: jnp.where(reached, a, b), new, before)

    return lax.fori_loop(0, length, lap, start)


def identity_state(head_count, head_dim):
    return (
        jnp.zeros((head_count, head_dim, head_dim), jnp.float32),
        jnp.zeros((head_count, head_dim), jnp.float32),
        jnp.full((head_count,), very_negative, jnp.float32),
        jnp.zeros((head_count,), jnp.float32),
        jnp.array(-1.0, jnp.float32),
        jnp.array(-1.0, jnp.float32),
    )


def combine(earlier, later):
    memory_one, normal_one, top_one, decay_one, first_one, last_one = earlier
    memory_two, normal_two, top_two, decay_two, first_two, last_two = later
    later_empty = first_two < 0.0
    earlier_empty = first_one < 0.0
    keep = later_empty | (first_two == last_two) & (first_two == last_one)
    decay_step = jnp.where(later_empty, 0.0, decay_two)
    top_new = jnp.where(keep, jnp.maximum(decay_step + top_one, top_two), top_two)
    scale_old = jnp.where(keep, jnp.exp(decay_step + top_one - top_new), 0.0)
    scale_new = jnp.exp(top_two - top_new)
    memory_new = scale_old[:, None, None] * memory_one + scale_new[:, None, None] * memory_two
    normal_new = scale_old[:, None] * normal_one + scale_new[:, None] * normal_two
    decay_new = jnp.where(keep, decay_one + decay_step, decay_two)
    first_new = jnp.where(earlier_empty, first_two, first_one)
    last_new = jnp.where(later_empty, last_one, last_two)
    return (memory_new, normal_new, top_new, decay_new, first_new, last_new)


def block_summary(key_block, value_block, gate_block, decay_block, segment):
    cumulative = jnp.cumsum(decay_block, axis=-1)
    latest = segment == segment[-1]
    growth = jnp.where(latest[None, :], cumulative[:, -1:] - cumulative + gate_block, very_negative)
    top_log = jnp.max(growth, axis=-1)
    weight_table = jnp.exp(growth - top_log[:, None])
    key_expanded = key_block.astype(jnp.float32)
    value_expanded = value_block.astype(jnp.float32)
    memory_matrix = jnp.einsum(
        "jw,wjm,wju->jmu",
        weight_table,
        key_expanded,
        value_expanded,
        precision=lax.Precision.HIGHEST,
    )
    normal = jnp.einsum("hs,shk->hk", weight_table, key_expanded, precision=lax.Precision.HIGHEST)
    return (memory_matrix, normal, top_log, cumulative[:, -1], segment[0], segment[-1])


def block_output(query_block, key_block, value_block, gate_block, decay_block, segment, state):
    memory_matrix, normal, top_log, total_decay, first_doc, last_doc = state
    head_dim = query_block.shape[2]
    length = segment.shape[0]
    cumulative = jnp.cumsum(decay_block, axis=-1)
    row_ids = lax.broadcasted_iota(jnp.int32, (length, length), 0)
    col_ids = lax.broadcasted_iota(jnp.int32, (length, length), 1)
    allowed = (col_ids <= row_ids) & (segment[:, None] == segment[None, :])
    inside = jnp.where(
        allowed[None],
        cumulative[:, :, None] - cumulative[:, None, :] + gate_block[:, None, :],
        very_negative,
    )
    outside = jnp.where(
        (segment == last_doc)[None, :], cumulative + top_log[:, None], very_negative
    )
    peak_log = jnp.maximum(outside, jnp.max(inside, axis=-1))
    carried = jnp.exp(outside - peak_log)
    scaled = query_block * jnp.asarray(head_dim ** (-0.5), query_block.dtype)
    scores = jnp.einsum("lhd,shd->hls", scaled, key_block, preferred_element_type=jnp.float32)
    weight_table = jnp.exp(inside - peak_log[:, :, None]) * scores
    from_block = jnp.einsum(
        "hls,shv->hlv",
        weight_table.astype(jnp.bfloat16),
        value_block,
        preferred_element_type=jnp.float32,
    )
    scaled_expanded = scaled.astype(jnp.float32)
    memory_readout = jnp.einsum(
        "pug,uga->upa", scaled_expanded, memory_matrix, precision=lax.Precision.HIGHEST
    )
    numer_part = carried[:, :, None] * memory_readout + from_block
    denom_part = carried * jnp.einsum(
        "lhk,hk->hl", scaled_expanded, normal, precision=lax.Precision.HIGHEST
    ) + jnp.sum(weight_table, axis=-1)
    result = numer_part / jnp.maximum(jnp.abs(denom_part), jnp.exp(-peak_log))[:, :, None]
    return jnp.transpose(result, (1, 0, 2)).reshape(length, -1).astype(jnp.bfloat16)


def on_device(
    residual,
    query_vectors,
    key_vectors,
    value_vectors,
    in_gate,
    forget_gate,
    documents,
    w_out,
    norm_gain,
    w_up,
    w_down,
):
    tok_rows = query_vectors.shape[0]
    local_heads = in_gate.shape[0]
    head_dim = query_vectors.shape[1] // local_heads
    block_count = tok_rows // SPAN

    def to_blocks(vectors):
        return vectors.reshape(block_count, SPAN, local_heads, head_dim)

    def gate_blocks(gates):
        return jnp.transpose(gates.reshape(local_heads, block_count, SPAN), (1, 0, 2))

    query_blocks = to_blocks(query_vectors)
    key_blocks = to_blocks(key_vectors)
    value_blocks = to_blocks(value_vectors)
    input_blocks = gate_blocks(in_gate)
    decay_blocks = gate_blocks(jax.nn.log_sigmoid(forget_gate))
    segments = documents.astype(jnp.float32).reshape(block_count, SPAN)
    summaries = jax.vmap(block_summary)(
        key_blocks, value_blocks, input_blocks, decay_blocks, segments
    )
    empty_state = identity_state(local_heads, head_dim)

    def prefix_step(state, summary):
        return (combine(state, summary), state)

    device_total, prefixes = lax.scan(prefix_step, empty_state, summaries)
    incoming = carried_in(device_total, "sp", combine, empty_state)
    entering = jax.vmap(combine, in_axes=(None, 0))(incoming, prefixes)
    mixed = jax.vmap(block_output)(
        query_blocks, key_blocks, value_blocks, input_blocks, decay_blocks, segments, entering
    )
    mixed = mixed.reshape(tok_rows, local_heads * head_dim)
    regrouped = lax.all_to_all(mixed, "tp", split_axis=0, concat_axis=1, tiled=True)
    columns = regrouped
    projected = jnp.dot(
        columns, lax.all_gather(w_out, "tp", axis=0, tiled=True), preferred_element_type=jnp.float32
    )
    middle = (residual.astype(jnp.float32) + projected).astype(jnp.bfloat16)
    middle_wide = middle.astype(jnp.float32)
    factor = lax.rsqrt(jnp.mean(middle_wide * middle_wide, axis=-1, keepdims=True) + epsilon)
    normed = (middle_wide * factor * norm_gain.astype(jnp.float32)).astype(jnp.bfloat16)
    gathered = lax.all_gather(normed, "tp", axis=0, tiled=True)
    columns = gathered
    lifted = jnp.dot(
        columns, lax.all_gather(w_up, "sp", axis=0, tiled=True), preferred_element_type=jnp.float32
    )
    hidden = jnp.square(jax.nn.relu(lifted)).astype(jnp.bfloat16)
    terms = jnp.dot(
        hidden, lax.all_gather(w_down, "sp", axis=1, tiled=True), preferred_element_type=jnp.float32
    )
    summed = lax.psum_scatter(
        terms.astype(jnp.bfloat16), "tp", scatter_dimension=0, tiled=True
    ).astype(jnp.float32)
    return (middle_wide + summed).astype(jnp.bfloat16)


def solution(mesh):
    placed = (
        P(("sp", "tp"), None),
        P("sp", "tp"),
        P("sp", "tp"),
        P("sp", "tp"),
        P("tp", "sp"),
        P("tp", "sp"),
        P("sp"),
        P("tp", None),
        P(),
        P("sp", "tp"),
        P("tp", "sp"),
    )
    return jax.shard_map(
        on_device, mesh=mesh, in_specs=placed, out_specs=P(("sp", "tp"), None), check_vma=False
    )
```

profile of v0, /device:TPU:0, one launch (start us, length us, event | category | flops | bytes accessed | tf_op | source)
XLA Modules:
  0.0 511.1 jit_solution(8846787200100752153)
XLA Ops:
  6.5 0.7 fusion.36
  8.1 0.7 convert_bitcast_fusion
  8.9 0.8 broadcast_compare_fusion.1
  9.7 0.8 fusion.42
  10.5 0.8 fusion.59
  11.3 0.8 subtract_exponential_fusion.2
  12.2 1.0 copy.53
  13.2 1.1 reshape.152
  15.3 11.2 %while.55 = (s32[]{:T(128)}, f32[4,64,64]{2,1,0:T(8,128)S(1)}, f32[4,64]{1,0:T(4,128)S(1)}, f32[4]{0:T(128)S(1)}, f32[4]{0:T(128)S(1)}, /*index=5*/f32[]{:T(128)...) while((s32[]{:T(128)}, f32[4,64,64]{2,1,0:T(8,128)S(1)}, ...), condition=%wide.region_3.4_spmd.clone.clone, body=%wide.region_2.3_spmd.clone.sunk.clone | while | flops 83255 | bytes 466630 | solution.py:153
  26.5 0.7 copy-done
  27.2 0.7 all-gather.11.cloned.1.call-update
  29.6 0.7 dynamic-update-slice
  30.2 0.7 dynamic-update-slice.1
  30.9 35.2 %all-reduce.4 = (f32[16]{0:T(128)S(1)}, f32[16]{0:T(128)S(1)}, f32[64]{0:T(128)S(1)}, f32[64]{0:T(128)S(1)}) all-reduce(f32[16]{0:T(128)S(1)} %dynamic-update-slice, f32[16]{0:T(128)S(1)} %dynamic-update-slice.1, f32[64]{0:T(128)S(1)} %dynamic-update-slice.2, f32[64]{0:T(128)S(1)} %dynamic-update-slice.3), channel_id=1, replica_groups=mesh['sp'=16,'tp'=2] {'sp'}, use_global_device_ids=true, to_apply=%add | all-reduce | flops 160 | bytes 1280
  66.3 17.2 %all-gather.4 = f32[16,4,64]{2,1,0:T(4,128)S(1)} all-gather(f32[1,4,64]{2,1,0:T(4,128)S(1)} %bitcast.198), channel_id=5, replica_groups=mesh['sp'=16,'tp'=2] {'sp'}, dimensions={0}, use_global_device_ids=true | all-gather | bytes 17408 | tf_op jit(solution)/shard_map/all_gather | solution.py:13
  84.4 91.4 %while.56 = (s32[]{:T(128)}, f32[4,64,64]{2,1,0:T(8,128)S(1)}, f32[4,64]{1,0:T(4,128)S(1)}, f32[4]{0:T(128)S(1)}, f32[]{:T(128)}, /*index=5*/s32[]{:T(128)}, f32...) while((s32[]{:T(128)}, f32[4,64,64]{2,1,0:T(8,128)S(1)}, ...), condition=%wide.region_5.6_spmd.clone.clone, body=%wide.region_4.5_spmd.clone.sunk.clone | while | flops 83247 | bytes 200163 | solution.py:25
  85.0 0.6 dynamic_slice.136
  88.3 1.0 fusion.70
  94.0 1.0 fusion.70
  96.4 0.6 dynamic_slice.136
  99.7 1.0 fusion.70
  102.1 0.6 dynamic_slice.136
  105.4 1.0 fusion.70
  111.2 1.0 fusion.70
  113.5 0.6 dynamic_slice.136
  116.9 1.0 fusion.70
  119.2 0.6 dynamic_slice.136
  122.6 1.0 fusion.70
  128.3 1.0 fusion.70
  134.0 1.0 fusion.70
  139.7 1.0 fusion.70
  145.4 1.0 fusion.70
  151.1 1.0 fusion.70
  156.8 1.0 fusion.70
  162.6 1.0 fusion.70
  168.3 1.0 fusion.70
  174.0 1.0 fusion.70
  177.4 0.9 fusion.21
  178.2 3.4 all-to-all-start
  181.7 4.5 all-to-all-done
  186.2 2.1 multiply_reduce_fusion
  188.3 1.0 multiply_convert_fusion
  190.5 18.0 %all-gather.13.cloned.1.call-done = bf16[256,2048]{1,0:T(8,128)(2,1)} async-done(((bf16[128,2048]{1,0:T(8,128)(2,1)}), bf16[256,2048]{1,0:T(8,128)(2,1)}) %all-gather.13.cloned.1.call-update) | async-done | bytes 1048592 | tf_op jit(solution)/shard_map/all_gather | solution.py:169
  208.5 128.5 %all-gather.15.cloned.1.call-done = bf16[2048,4096]{1,0:T(8,128)(2,1)} async-done(((bf16[128,4096]{1,0:T(8,128)(2,1)}), bf16[2048,4096]{1,0:T(8,128)(2,1)}) %all-gather.15.cloned.1.call-update) | async-done | bytes 16777232 | tf_op jit(solution)/shard_map/all_gather | solution.py:172
  337.0 130.1 %all-gather.17.cloned.1.call-done = bf16[4096,2048]{1,0:T(8,128)(2,1)} async-done(((bf16[4096,128]{1,0:T(8,128)(2,1)}), bf16[4096,2048]{1,0:T(8,128)(2,1)}) %all-gather.17.cloned.1.call-update) | async-done | bytes 16777232 | tf_op jit(solution)/shard_map/all_gather | solution.py:176
  467.1 16.5 %convolution_convert_fusion = bf16[256,2048]{1,0:T(8,128)(2,1)} fusion(bf16[4096,2048]{1,0:T(8,128)(2,1)} %all-gather.17.cloned.1.call-done, bf16[256,2048]{1,0:T(8,128)(2,1)} %all-gather.13.cloned.1.call-done, bf16[2048,4096]{1,0:T(8,128)(2,1)} %all-gather.15.cloned.1.call-done), kind=kOutput, calls=%fused_computation.40 | convolution fusion | flops 8593604608 | bytes 35651584 | tf_op jit(solution)/shard_map/dot_general | solution.py:175
  483.6 18.7 %reduce-scatter.2.cloned.1.call-done = bf16[128,2048]{1,0:T(8,128)(2,1)} async-done(((bf16[256,2048]{1,0:T(8,128)(2,1)}), bf16[128,2048]{1,0:T(8,128)(2,1)}) %reduce-scatter.2.cloned.1.call-update) | async-done | bytes 524304 | tf_op jit(solution)/shard_map/reduce_scatter | solution.py:178
  502.3 2.0 add_convert_fusion
  (177 shorter events, 28.8 us)
Async XLA Ops:
  6.5 21.5 %copy-start.6 = (u32[32]{0:T(128)S(1)}, u32[32]{0:T(128)}, u32[]{:S(2)}) copy-start(u32[32]{0:T(128)} %constant.91) | copy-start | bytes 388
  6.5 77.0 %copy-start.2 = (bf16[256,256]{1,0:T(8,128)(2,1)S(1)}, bf16[256,256]{1,0:T(8,128)(2,1)}, u32[]{:S(2)}) copy-start(bf16[256,256]{1,0:T(8,128)(2,1)} %param.16) | copy-start | bytes 393220
  6.5 77.8 %all-gather.19.cloned.1.call-start = ((), (), s32[]{:S(2)}) async-start(), calls=%async_computation.7 | async-start | bytes 2228224 | tf_op jit(solution)/shard_map/all_gather | solution.py:13
  13.2 70.8 %copy-start.3 = (f32[4,256]{1,0:T(4,128)S(1)}, f32[4,256]{1,0:T(4,128)}, u32[]{:S(2)}) copy-start(f32[4,256]{1,0:T(4,128)} %param.19) | copy-start | bytes 12292
  15.2 160.6 %copy-start.4 = (s32[256]{0:T(256)S(1)}, s32[256]{0:T(256)}, u32[]{:S(2)}) copy-start(s32[256]{0:T(256)} %param.21) | copy-start | bytes 3076
  26.5 0.7 copy-start
  27.2 154.5 %copy-start.5 = (bf16[2048]{0:T(1024)(128)(2,1)S(1)}, bf16[2048]{0:T(1024)(128)(2,1)}, u32[]{:S(2)}) copy-start(bf16[2048]{0:T(1024)(128)(2,1)} %param.23) | copy-start | bytes 12292
  27.2 159.0 %copy-start.1 = (bf16[128,2048]{1,0:T(8,128)(2,1)S(1)}, bf16[128,2048]{1,0:T(8,128)(2,1)}, u32[]{:S(2)}) copy-start(bf16[128,2048]{1,0:T(8,128)(2,1)} %param.15) | copy-start | bytes 1572868
  27.2 159.0 %all-gather.11.cloned.1.call-start = ((), (), s32[]{:S(2)}) async-start(), calls=%async_computation.2 | async-start | bytes 3145728 | tf_op jit(solution)/shard_map/all_gather | solution.py:163
  178.2 7.9 %all-to-all-start = ((bf16[2,128,256]{1,2,0:T(8,128)(2,1)}), bf16[2,128,256]{1,2,0:T(8,128)(2,1)S(1)}, u32[]{:S(2)}, u32[]{:S(2)}) async-start(bf16[2,128,256]{1,2,0:T(8,128)(2,1)} %bitcast.27), calls=%async_computation | async-start | bytes 262144 | tf_op jit(solution)/shard_map/all_to_all | solution.py:160
  181.6 26.9 %all-gather.13.cloned.1.call-start = ((), (), s32[]{:S(2)}) async-start(), calls=%async_computation.3 | async-start | bytes 1572864 | tf_op jit(solution)/shard_map/all_gather | solution.py:169
  189.3 147.7 %all-gather.15.cloned.1.call-start = ((), (), s32[]{:S(2)}) async-start(), calls=%async_computation.4 | async-start | bytes 17825792 | tf_op jit(solution)/shard_map/all_gather | solution.py:172
  189.9 277.2 %all-gather.17.cloned.1.call-start = ((), (), s32[]{:S(2)}) async-start(), calls=%async_computation.5 | async-start | bytes 17825792 | tf_op jit(solution)/shard_map/all_gather | solution.py:176
  190.5 311.8 %reduce-scatter.2.cloned.1.call-start = ((), (), s32[]{:S(2)}) async-start(), calls=%async_computation.6 | async-start | bytes 1572864 | tf_op jit(solution)/shard_map/reduce_scatter | solution.py:178
Sparse Core Ops, SparseCore 0:
  27.3 44.1 all-gather.18
  73.0 31.7 all-gather.10
  189.4 19.0 all-gather.12
  210.5 126.4 all-gather.14
  339.0 128.0 all-gather.16
  483.7 18.5 reduce-scatter.1
where the time goes:
time: 513 us; the launch traced here: 511 us
  waiting for transfers between devices  302 us (59%)
  loops' own time  61.4 us (12%)
  blocking collectives  52.5 us (10%)
  local copies, waits for them, and re-layouts  28.9 us (6%)
  other arithmetic  27.6 us (5%)
  matrix products  21.3 us (4%)
  between operations  14.4 us (3%)
    all_gather x1, waiting for transfers between devices, on_device(): lax.all_gather(w_down, 'sp', axis=1, tiled=True)  130 us
    all_gather x1, waiting for transfers between devices, on_device(): lax.all_gather(w_up, 'sp', axis=0, tiled=True)  128 us
    another operation x1, loops' own time, carried_in(): return lax.fori_loop(0, length, lap, start)  53.6 us
    unnamed x1, blocking collectives  35.2 us
    dynamic_slice x32, local copies, waits for them, and re-layouts, lap(): new = combine(before, jax.tree.map(lambda part: part[k], everything))  19.7 us
    reduce_scatter x1, waiting for transfers between devices, on_device(): lax.psum_scatter(terms.astype(jnp.bfloat16), 'tp', scatter_dimension=0, t...  18.7 us
    all_gather x1, waiting for transfers between devices, on_device(): gathered = lax.all_gather(normed, 'tp', axis=0, tiled=True)  18 us
    select_n x48, other arithmetic, lap(): return jax.tree.map(lambda a, b: jnp.where(reached, a, b), new, before)  17.7 us
  transfers between devices with their start and end apart: 7, of which 5 were waited for; matrix products, arithmetic and copies ran while one was open for 9% of the time, Pallas kernels for 0%

commit v1 on v0

--- a/solution.py
+++ b/solution.py
@@ -2,10 +2,12 @@
 import jax.numpy as jnp
 from jax import lax
 from jax.sharding import PartitionSpec as P
+from jax.lax import all_gather
 
 SPAN = 128
 very_negative = -1e30
 epsilon = 1e-06
+_return_all_chunk = lambda v0: jnp.concatenate(all_gather(v0, axis_name="sp"), axis=1)
 
 
 def carried_in(value, axis, combine, identity):
@@ -172,9 +174,7 @@
         columns, lax.all_gather(w_up, "sp", axis=0, tiled=True), preferred_element_type=jnp.float32
     )
     hidden = jnp.square(jax.nn.relu(lifted)).astype(jnp.bfloat16)
-    terms = jnp.dot(
-        hidden, lax.all_gather(w_down, "sp", axis=1, tiled=True), preferred_element_type=jnp.float32
-    )
+    terms = jnp.dot(hidden, _return_all_chunk(w_down), preferred_element_type=jnp.float32)
     summed = lax.psum_scatter(
         terms.astype(jnp.bfloat16), "tp", scatter_dimension=0, tiled=True
     ).astype(jnp.float32)

time: 513 us -> 429 us (0.84)
  waiting for transfers between devices: 302 us -> 202 us
  local copies, waits for them, and re-layouts: 28.9 us -> 49 us
    all_gather x1, waiting for transfers between devices: 130 us -> 48.2 us  [all_gather(v0, axis_name='sp')]
    reshape x0 -> x1, local copies, waits for them, and re-layouts: none -> 21.3 us  [jnp.concatenate(all_gather(v0, axis_name='sp'), axis=1)]
    all_gather x1, waiting for transfers between devices: 18 us -> 0.01 us  [on_device(): gathered = lax.all_gather(normed, 'tp', axis=0, tiled=True)]
  transfers between devices with their start and end apart: 7 -> 7, of which waited for: 5 -> 4; matrix products, arithmetic and copies ran while one was open for 9% -> 16% of each run, Pallas kernels for 0% -> 0%
where the time goes in v1:
time: 429 us; the launch traced here: 427 us
  waiting for transfers between devices  202 us (47%)
  loops' own time  57.1 us (13%)
  blocking collectives  52.4 us (12%)
  local copies, waits for them, and re-layouts  49 us (11%)
  other arithmetic  27.6 us (6%)
  matrix products  21.3 us (5%)
  between operations  14.5 us (3%)
    all_gather x1, waiting for transfers between devices, on_device(): lax.all_gather(w_up, 'sp', axis=0, tiled=True)  128 us
    another operation x1, loops' own time, carried_in(): return lax.fori_loop(0, length, lap, start)  49.4 us
    all_gather x1, waiting for transfers between devices, all_gather(v0, axis_name='sp')  48.2 us
    unnamed x1, blocking collectives  35.2 us
    reshape x1, local copies, waits for them, and re-layouts, jnp.concatenate(all_gather(v0, axis_name='sp'), axis=1)  21.3 us
    reduce_scatter x1, waiting for transfers between devices, on_device(): lax.psum_scatter(terms.astype(jnp.bfloat16), 'tp', scatter_dimension=0, t...  18.7 us
    dynamic_slice x32, local copies, waits for them, and re-layouts, lap(): new = combine(before, jax.tree.map(lambda part: part[k], everything))  18.2 us
    select_n x48, other arithmetic, lap(): return jax.tree.map(lambda a, b: jnp.where(reached, a, b), new, before)  17.8 us
  transfers between devices with their start and end apart: 7, of which 4 were waited for; matrix products, arithmetic and copies ran while one was open for 16% of the time, Pallas kernels for 0%

profile of v1, /device:TPU:0, one launch (start us, length us, event | category | flops | bytes accessed | tf_op | source)
XLA Modules:
  0.0 427.0 jit_solution(16880081216858877177)
XLA Ops:
  6.5 0.7 fusion.36
  7.2 0.6 reduce_window_sum.12
  8.0 0.7 convert_bitcast_fusion
  8.9 0.8 broadcast_compare_fusion.1
  9.7 0.8 fusion.42
  10.5 0.8 fusion.59
  11.3 0.8 subtract_exponential_fusion.2
  12.1 1.0 copy.54
  13.2 1.1 reshape.161
  15.3 11.2 %while.55 = (s32[]{:T(128)}, f32[4,64,64]{2,1,0:T(8,128)S(1)}, f32[4,64]{1,0:T(4,128)S(1)}, f32[4]{0:T(128)S(1)}, f32[4]{0:T(128)S(1)}, /*index=5*/f32[]{:T(128)...) while((s32[]{:T(128)}, f32[4,64,64]{2,1,0:T(8,128)S(1)}, ...), condition=%wide.region_3.4_spmd.clone.clone, body=%wide.region_2.3_spmd.clone.sunk.clone | while | flops 83255 | bytes 466630 | solution.py:155
  15.3 0.6 dynamic_slice.131
  20.9 0.6 dynamic_slice.131
  26.5 0.7 copy-done
  27.2 0.7 all-gather.12.cloned.1.call-update
  28.0 0.7 all-gather.20.cloned.1.call-update
  28.7 0.6 dynamic-slice
  30.5 0.8 dynamic-update-slice
  31.3 0.8 dynamic-update-slice.1
  32.1 35.2 %all-reduce.4 = (f32[16]{0:T(128)S(1)}, f32[16]{0:T(128)S(1)}, f32[64]{0:T(128)S(1)}, f32[64]{0:T(128)S(1)}) all-reduce(f32[16]{0:T(128)S(1)} %dynamic-update-slice, f32[16]{0:T(128)S(1)} %dynamic-update-slice.1, f32[64]{0:T(128)S(1)} %dynamic-update-slice.2, f32[64]{0:T(128)S(1)} %dynamic-update-slice.3), channel_id=1, replica_groups=mesh['sp'=16,'tp'=2] {'sp'}, use_global_device_ids=true, to_apply=%add | all-reduce | flops 160 | bytes 1280
  67.8 17.2 %all-gather.5 = f32[16,4,64]{2,1,0:T(4,128)S(1)} all-gather(f32[1,4,64]{2,1,0:T(4,128)S(1)} %bitcast.204), channel_id=5, replica_groups=mesh['sp'=16,'tp'=2] {'sp'}, dimensions={0}, use_global_device_ids=true | all-gather | bytes 17408 | tf_op jit(solution)/shard_map/all_gather | solution.py:15
  85.5 85.6 %while.56 = (s32[]{:T(128)}, f32[4,64,64]{2,1,0:T(8,128)S(1)}, f32[4,64]{1,0:T(4,128)S(1)}, f32[4]{0:T(128)S(1)}, f32[]{:T(128)}, /*index=5*/s32[]{:T(128)}, f32...) while((s32[]{:T(128)}, f32[4,64,64]{2,1,0:T(8,128)S(1)}, ...), condition=%wide.region_5.6_spmd.clone.clone, body=%wide.region_4.5_spmd.clone.sunk.clone | while | flops 83247 | bytes 200163 | solution.py:27
  89.2 1.0 fusion.70
  94.5 1.0 fusion.70
  99.9 1.0 fusion.70
  105.2 1.0 fusion.70
  110.6 1.0 fusion.70
  115.9 1.0 fusion.70
  121.3 1.0 fusion.70
  126.6 1.0 fusion.70
  132.0 1.0 fusion.70
  137.3 1.0 fusion.70
  142.6 1.0 fusion.70
  148.0 1.0 fusion.70
  153.3 1.0 fusion.70
  158.7 1.1 fusion.70
  164.1 1.0 fusion.70
  169.4 1.0 fusion.70
  172.7 0.9 fusion.21
  173.6 3.4 all-to-all-start
  177.0 4.5 %all-to-all-done = bf16[2,128,256]{1,2,0:T(8,128)(2,1)S(1)} async-done(((bf16[2,128,256]{1,2,0:T(8,128)(2,1)}), bf16[2,128,256]{1,2,0:T(8,128)(2,1)S(1)}, u32[]{:S(2)}, u32[]{:S(2)}) %all-to-all-start) | async-done | bytes 131104 | tf_op jit(solution)/shard_map/all_to_all | solution.py:162
  181.5 2.1 multiply_reduce_fusion
  183.7 1.0 multiply_convert_fusion
  185.3 48.2 %all-gather.20.cloned.1.call-done = bf16[65536,128]{1,0:T(8,128)(2,1)} async-done(((bf16[4096,128]{1,0:T(8,128)(2,1)}), bf16[65536,128]{1,0:T(8,128)(2,1)}) %all-gather.20.cloned.1.call-update) | async-done | bytes 16777232 | tf_op jit(solution)/shard_map/all_gather | solution.py:10
  233.5 21.3 %copy.65 = bf16[4096,16,128]{0,2,1:T(8,128)(2,1)} copy(bf16[4096,16,128]{2,0,1:T(8,128)(2,1)} %bitcast.201) | data formatting | bytes 33554432 | tf_op jit(solution)/shard_map/reshape | solution.py:10
  254.8 128.1 %all-gather.16.cloned.1.call-done = bf16[2048,4096]{1,0:T(8,128)(2,1)} async-done(((bf16[128,4096]{1,0:T(8,128)(2,1)}), bf16[2048,4096]{1,0:T(8,128)(2,1)}) %all-gather.16.cloned.1.call-update) | async-done | bytes 16777232 | tf_op jit(solution)/shard_map/all_gather | solution.py:174
  383.0 16.5 %convolution_convert_fusion = bf16[256,2048]{1,0:T(8,128)(2,1)} fusion(bf16[4096,2048]{0,1:T(8,128)(2,1)} %bitcast.202, bf16[256,2048]{1,0:T(8,128)(2,1)} %all-gather.14.cloned.1.call-done, bf16[2048,4096]{1,0:T(8,128)(2,1)} %all-gather.16.cloned.1.call-done), kind=kOutput, calls=%fused_computation.40 | convolution fusion | flops 8593604608 | bytes 35651584 | tf_op jit(solution)/shard_map/dot_general | solution.py:177
  399.4 18.7 %reduce-scatter.2.cloned.1.call-done = bf16[128,2048]{1,0:T(8,128)(2,1)} async-done(((bf16[256,2048]{1,0:T(8,128)(2,1)}), bf16[128,2048]{1,0:T(8,128)(2,1)}) %reduce-scatter.2.cloned.1.call-update) | async-done | bytes 524304 | tf_op jit(solution)/shard_map/reduce_scatter | solution.py:178
  418.2 2.0 add_convert_fusion
  (178 shorter events, 27.6 us)
Async XLA Ops:
  6.5 78.9 %all-gather.18.cloned.1.call-start = ((), (), s32[]{:S(2)}) async-start(), calls=%async_computation.6 | async-start | bytes 2228224 | tf_op jit(solution)/shard_map/all_gather | solution.py:15
  13.1 15.6 %copy-start.6 = (u32[32]{0:T(128)S(1)}, u32[32]{0:T(128)}, u32[]{:S(2)}) copy-start(u32[32]{0:T(128)} %constant.91) | copy-start | bytes 388
  13.1 54.3 %copy-start.2 = (bf16[256,256]{1,0:T(8,128)(2,1)S(1)}, bf16[256,256]{1,0:T(8,128)(2,1)}, u32[]{:S(2)}) copy-start(bf16[256,256]{1,0:T(8,128)(2,1)} %param.16) | copy-start | bytes 393220
  14.6 70.5 %copy-start.3 = (f32[4,256]{1,0:T(4,128)S(1)}, f32[4,256]{1,0:T(4,128)}, u32[]{:S(2)}) copy-start(f32[4,256]{1,0:T(4,128)} %param.19) | copy-start | bytes 12292
  15.2 155.9 %copy-start.4 = (s32[256]{0:T(256)S(1)}, s32[256]{0:T(256)}, u32[]{:S(2)}) copy-start(s32[256]{0:T(256)} %param.21) | copy-start | bytes 3076
  26.5 0.7 copy-start
  27.2 154.3 %all-gather.12.cloned.1.call-start = ((), (), s32[]{:S(2)}) async-start(), calls=%async_computation.2 | async-start | bytes 3145728 | tf_op jit(solution)/shard_map/all_gather | solution.py:165
  27.9 149.1 %copy-start.5 = (bf16[2048]{0:T(1024)(128)(2,1)S(1)}, bf16[2048]{0:T(1024)(128)(2,1)}, u32[]{:S(2)}) copy-start(bf16[2048]{0:T(1024)(128)(2,1)} %param.23) | copy-start | bytes 12292
  27.9 153.6 %copy-start.1 = (bf16[128,2048]{1,0:T(8,128)(2,1)S(1)}, bf16[128,2048]{1,0:T(8,128)(2,1)}, u32[]{:S(2)}) copy-start(bf16[128,2048]{1,0:T(8,128)(2,1)} %param.15) | copy-start | bytes 1572868
  28.0 205.6 %all-gather.20.cloned.1.call-start = ((), (), s32[]{:S(2)}) async-start(), calls=%async_computation.7 | async-start | bytes 17825792 | tf_op jit(solution)/shard_map/all_gather | solution.py:10
  173.6 7.9 %all-to-all-start = ((bf16[2,128,256]{1,2,0:T(8,128)(2,1)}), bf16[2,128,256]{1,2,0:T(8,128)(2,1)S(1)}, u32[]{:S(2)}, u32[]{:S(2)}) async-start(bf16[2,128,256]{1,2,0:T(8,128)(2,1)} %bitcast.27), calls=%async_computation | async-start | bytes 262144 | tf_op jit(solution)/shard_map/all_to_all | solution.py:162
  177.0 77.9 %all-gather.14.cloned.1.call-start = ((), (), s32[]{:S(2)}) async-start(), calls=%async_computation.3 | async-start | bytes 1572864 | tf_op jit(solution)/shard_map/all_gather | solution.py:171
  184.6 198.3 %all-gather.16.cloned.1.call-start = ((), (), s32[]{:S(2)}) async-start(), calls=%async_computation.4 | async-start | bytes 17825792 | tf_op jit(solution)/shard_map/all_gather | solution.py:174
  185.2 232.9 %reduce-scatter.2.cloned.1.call-start = ((), (), s32[]{:S(2)}) async-start(), calls=%async_computation.5 | async-start | bytes 1572864 | tf_op jit(solution)/shard_map/reduce_scatter | solution.py:178
Sparse Core Ops, SparseCore 0:
  27.3 44.2 all-gather.17
  73.1 31.8 all-gather.11
  107.1 126.3 all-gather.19
  234.9 19.5 all-gather.13
  256.5 126.4 all-gather.15
  399.6 18.5 reduce-scatter.1
